TPU v7x, 32 devices: a whole 2x2x4 slice. The times are simulated.
32 devices in a mesh: fs: 4 (over y, x), tp: 8 (over z, core).
Axes of the slice: x: 2, y: 2, z: 4, core: 2. Of those that a mesh axis runs over, the one named last changes fastest.
Arguments:
- normed_inputs: bfloat16 [4096, 4096], P('fs', 'tp'), may hold values from -6 to 6
- query_upstream: bfloat16 [4096, 4096], P('fs', 'tp'), may hold values from -0.125 to 0.125
- key_upstream: bfloat16 [4096, 1024], P('fs', 'tp'), may hold values from -0.09375 to 0.09375
- head_outputs: bfloat16 [4096, 4096], P('fs', 'tp'), may hold values from -6 to 6
- branch_upstream: bfloat16 [4096, 4096], P('fs', 'tp'), may hold values from -0.125 to 0.125
- query_master: float32 [4096, 4096], P('fs', 'tp'), may hold values from -0.09375 to 0.09375
- key_master: float32 [4096, 1024], P('fs', 'tp'), may hold values from -0.09375 to 0.09375
- branch_master: float32 [4096, 4096], P('fs', 'tp'), may hold values from -0.09375 to 0.09375
- query_basis: bfloat16 [4096, 128], replicated, may hold values from -0.09375 to 0.09375
- key_basis: bfloat16 [4096, 128], replicated, may hold values from -0.09375 to 0.09375
- branch_basis: bfloat16 [4096, 128], replicated, may hold values from -0.09375 to 0.09375
- query_first: float32 [128, 4096], P(None, 'tp'), may hold values from -0.75 to 0.75
- query_second: float32 [128, 4096], P(None, 'tp'), may hold values from 0.001 to 0.02
- key_first: float32 [128, 1024], P(None, 'tp'), may hold values from -0.75 to 0.75
- key_second: float32 [128, 1024], P(None, 'tp'), may hold values from 0.001 to 0.02
- branch_first: float32 [4096, 128], P('fs'), may hold values from -0.75 to 0.75
- branch_second: float32 [4096, 128], P('fs'), may hold values from 0.001 to 0.02
Outputs:
- query_step: float32 [4096, 4096], P('fs', 'tp')
- key_step: float32 [4096, 1024], P('fs', 'tp')
- branch_step: float32 [4096, 4096], P('fs', 'tp')
- query_updated: float32 [4096, 4096], P('fs', 'tp')
- key_updated: float32 [4096, 1024], P('fs', 'tp')
- branch_updated: float32 [4096, 4096], P('fs', 'tp')
- query_copy: bfloat16 [4096, 4096], P(None, 'tp')
- key_copy: bfloat16 [4096, 1024], P(None, 'tp')
- branch_copy: bfloat16 [4096, 4096], P(None, 'tp')
- query_first_new: float32 [128, 4096], P(None, 'tp')
- query_second_new: float32 [128, 4096], P(None, 'tp')
- key_first_new: float32 [128, 1024], P(None, 'tp')
- key_second_new: float32 [128, 1024], P(None, 'tp')
- branch_first_new: float32 [4096, 128], P('fs')
- branch_second_new: float32 [4096, 128], P('fs')
All inputs are finite; a program needn't handle non-finite values.
Results may differ from a plain program's by a relative error of at most 0.001.
Values may be sent and summed in bfloat16 or wider, within the bound.
No kernel may reach another device: no remote copies, remote signals or barrier semaphores. Data moves between devices by JAX's collectives and lax.ppermute only.
A program may use at most 128 MiB of HBM per device.

v0:
```python
import jax
import jax.numpy as jnp
from jax import lax
from jax.sharding import PartitionSpec as P

LEARN = 0.02
BETA_ONE = 0.9
BETA_TWO = 0.95
ADAM_EPS = 1e-08
CLIP_RMS = 0.5


def moments(first, second, low, clip):
    scaled = clip * low
    first_new = BETA_ONE * first + (1.0 - BETA_ONE) * scaled
    second_new = BETA_TWO * second + (1.0 - BETA_TWO) * scaled * scaled
    return (first_new, second_new, first_new / (jnp.sqrt(second_new) + ADAM_EPS))


def over_tokens(left, right, precision=None):
    return lax.dot_general(
        left,
        right,
        (((0,), (0,)), ((), ())),
        precision=precision,
        preferred_element_type=jnp.float32,
    )


def per_device(
    normed_inputs,
    query_upstream,
    key_upstream,
    head_outputs,
    branch_upstream,
    query_master,
    key_master,
    branch_master,
    query_basis,
    key_basis,
    branch_basis,
    query_first,
    query_second,
    key_first,
    key_second,
    branch_first,
    branch_second,
):
    exact = lax.Precision.HIGHEST
    row_index = lax.axis_index("fs")
    col_index = lax.axis_index("tp")
    n_rows = lax.axis_size("fs")
    n_cols = lax.axis_size("tp")
    features = normed_inputs.shape[1]
    query_local = query_upstream.shape[1]
    key_local = key_upstream.shape[1]
    rows_in = query_master.shape[0]
    rank = query_basis.shape[1]
    whole_values = lax.all_gather(head_outputs, "tp", axis=1, tiled=True)
    block_query = lax.dynamic_slice_in_dim(query_basis, col_index * features, features, 0)
    block_key = lax.dynamic_slice_in_dim(key_basis, col_index * features, features, 0)
    proj_query, proj_key = lax.psum(
        (
            jnp.dot(normed_inputs, block_query, preferred_element_type=jnp.float32),
            jnp.dot(normed_inputs, block_key, preferred_element_type=jnp.float32),
        ),
        "tp",
    )
    part_query = over_tokens(proj_query, query_upstream.astype(jnp.float32), exact)
    part_key = over_tokens(proj_key, key_upstream.astype(jnp.float32), exact)
    grad_branch = lax.psum_scatter(
        over_tokens(whole_values, branch_upstream), "fs", scatter_dimension=0, tiled=True
    )
    own_branch = lax.dynamic_slice_in_dim(branch_basis, col_index * features, features, 0).astype(
        jnp.float32
    )
    part_branch = jnp.dot(grad_branch, own_branch, precision=exact)
    query_low, key_low = lax.psum((part_query, part_key), "fs")
    branch_low = lax.psum(part_branch, "tp")
    local_squares = (jnp.sum(query_low * query_low) + jnp.sum(key_low * key_low)) / n_rows
    local_squares = local_squares + jnp.sum(branch_low * branch_low) / n_cols
    total = lax.psum(local_squares, ("fs", "tp"))
    entries = rank * n_cols * (2 * query_local + key_local)
    rms_value = jnp.sqrt(total / float(entries))
    clip = 1.0 / jnp.maximum(1.0, rms_value / CLIP_RMS)
    q_first, q_second, q_dir = moments(query_first, query_second, query_low, clip)
    k_first, k_second, k_dir = moments(key_first, key_second, key_low, clip)
    b_first, b_second, b_dir = moments(branch_first, branch_second, branch_low, clip)
    step_rows_query = lax.dynamic_slice_in_dim(query_basis, row_index * rows_in, rows_in, 0).astype(
        jnp.float32
    )
    step_rows_key = lax.dynamic_slice_in_dim(key_basis, row_index * rows_in, rows_in, 0).astype(
        jnp.float32
    )
    query_step = jnp.dot(step_rows_query, q_dir, precision=exact)
    key_step = jnp.dot(step_rows_key, k_dir, precision=exact)
    branch_step = jnp.dot(b_dir, own_branch.T, precision=exact)
    query_updated = query_master - LEARN * query_step
    key_updated = key_master - LEARN * key_step
    branch_updated = branch_master - LEARN * branch_step
    query_copy, key_copy, branch_copy = (
        lax.all_gather(query_updated.astype(jnp.bfloat16), "fs", axis=0, tiled=True),
        lax.all_gather(key_updated.astype(jnp.bfloat16), "fs", axis=0, tiled=True),
        lax.all_gather(branch_updated.astype(jnp.bfloat16), "fs", axis=0, tiled=True),
    )
    return (
        query_step,
        key_step,
        branch_step,
        query_updated,
        key_updated,
        branch_updated,
        query_copy,
        key_copy,
        branch_copy,
        q_first,
        q_second,
        k_first,
        k_second,
        b_first,
        b_second,
    )


def solution(mesh):
    return jax.shard_map(
        per_device,
        mesh=mesh,
        in_specs=(
            P("fs", "tp"),
            P("fs", "tp"),
            P("fs", "tp"),
            P("fs", "tp"),
            P("fs", "tp"),
            P("fs", "tp"),
            P("fs", "tp"),
            P("fs", "tp"),
            P(),
            P(),
            P(),
            P(None, "tp"),
            P(None, "tp"),
            P(None, "tp"),
            P(None, "tp"),
            P("fs", None),
            P("fs", None),
        ),
        out_specs=(
            P("fs", "tp"),
            P("fs", "tp"),
            P("fs", "tp"),
            P("fs", "tp"),
            P("fs", "tp"),
            P("fs", "tp"),
            P(None, "tp"),
            P(None, "tp"),
            P(None, "tp"),
            P(None, "tp"),
            P(None, "tp"),
            P(None, "tp"),
            P(None, "tp"),
            P("fs", None),
            P("fs", None),
        ),
        check_vma=False,
    )
```

profile of v0, /device:TPU:0, one launch (start us, length us, event | category | flops | bytes accessed | tf_op | source)
XLA Modules:
  0.0 502.3 jit_solution(1356573704103843505)
XLA Ops:
  7.2 0.0 copy-start
  7.2 0.0 all-gather.5.cloned.1.call-start
  7.2 0.7 all-gather.5.cloned.1.call-update
  7.9 0.0 reduce-scatter.2.cloned.1.call-start
  8.0 86.4 %all-gather.5.cloned.1.call-done = bf16[1024,4096]{1,0:T(8,128)(2,1)} async-done(((bf16[1024,512]{1,0:T(8,128)(2,1)}), bf16[1024,4096]{1,0:T(8,128)(2,1)}) %all-gather.5.cloned.1.call-update) | async-done | bytes 8388624 | tf_op jit(solution)/shard_map/all_gather | solution.py:59
  94.4 10.4 %fusion.39 = f32[4096,512]{1,0:T(8,128)} fusion(bf16[1024,4096]{1,0:T(8,128)(2,1)} %all-gather.5.cloned.1.call-done, bf16[1024,512]{1,0:T(8,128)(2,1)S(1)} %copy-done), kind=kOutput, calls=%fused_computation.53 | convolution fusion | flops 4294967296 | bytes 17825792 | tf_op jit(solution)/shard_map/dot_general | solution.py:21
  104.9 0.0 reduce-scatter.2.cloned.1.call-update
  104.9 0.0 all-reduce.5.cloned.1.call-start
  104.9 1.1 copy-done.2
  106.1 2.2 convolution_bitcast_fusion
  108.2 2.2 convolution_bitcast_fusion.1
  110.4 79.4 %reduce-scatter.2.cloned.1.call-done = f32[1024,512]{1,0:T(8,128)} async-done(((f32[4096,512]{1,0:T(8,128)}), f32[1024,512]{1,0:T(8,128)}) %reduce-scatter.2.cloned.1.call-update) | async-done | bytes 2097168 | tf_op jit(solution)/shard_map/reduce_scatter | solution.py:71
  189.8 3.4 fusion.18
  193.3 0.0 all-reduce.5.cloned.1.call-update
  193.3 0.0 all-reduce.7.cloned.1.call-start
  193.4 62.4 %all-reduce.5.cloned.1.call-done = (f32[1024,128]{0,1:T(8,128)}, f32[1024,128]{0,1:T(8,128)}, f32[1024,128]{1,0:T(8,128)}) async-done(((f32[1024,128]{0,1:T(8,128)}, f32[1024,128]{0,1:T(8,128)}, f32[1024,128]{1,0:T(8,128)}), (f32[1024,128]{0,1:T(8,128)}, f32[1024,128]{0,1:T(8,128)}, f32[1024,128]{1,0:T(8,128)})) %all-reduce.5.cloned.1.call-update) | async-done | bytes 1572880 | tf_op jit(solution)/shard_map/psum | solution.py:62
  255.8 2.5 fusion.37
  258.3 1.0 fusion.38
  259.3 0.0 all-reduce.7.cloned.1.call-update
  259.3 0.0 all-gather.9.cloned.1.call-start
  259.4 0.7 multiply_reduce_fusion
  260.7 41.6 %all-reduce.7.cloned.1.call-done = (f32[128,512]{1,0:T(8,128)}, f32[128,128]{1,0:T(8,128)}) async-done(((f32[128,512]{1,0:T(8,128)}, f32[128,128]{1,0:T(8,128)}), (f32[128,512]{1,0:T(8,128)}, f32[128,128]{1,0:T(8,128)})) %all-reduce.7.cloned.1.call-update) | async-done | bytes 327696 | tf_op jit(solution)/shard_map/psum | solution.py:78
  302.3 1.6 multiply_reduce_fusion.1
  303.9 1.5 multiply_reduce_fusion.2
  306.7 39.3 %psum.47 = f32[]{:T(128)} all-reduce(f32[]{:T(128)S(6)} %add.68), channel_id=1, replica_groups=mesh['fs'=4,'tp'=8] {'fs','tp'}, use_global_device_ids=true, to_apply=%region_9.0 | all-reduce | flops 1 | bytes 8 | tf_op jit(solution)/shard_map/psum | solution.py:82
  346.8 0.9 fusion.20
  347.6 0.0 copy-start.17
  347.7 2.6 fusion.35
  350.2 0.0 all-gather.9.cloned.1.call-update
  350.3 0.0 all-gather.11.cloned.1.call-start
  350.3 1.4 fusion
  351.7 0.0 copy-start.4
  351.7 0.0 copy-start.5
  351.7 4.7 fusion.34
  356.4 0.0 all-gather.11.cloned.1.call-update
  356.4 0.0 all-gather.7.cloned.1.call-start
  356.5 1.2 fusion.5
  357.7 0.0 copy-start.9
  357.7 0.0 copy-start.10
  357.7 0.4 copy-done.8
  358.1 4.5 fusion.36
  362.7 0.0 all-gather.7.cloned.1.call-update
  362.7 15.2 %all-gather.9.cloned.1.call-done = bf16[4096,128]{1,0:T(8,128)(2,1)} async-done(((bf16[1024,128]{1,0:T(8,128)(2,1)}), bf16[4096,128]{1,0:T(8,128)(2,1)}) %all-gather.9.cloned.1.call-update) | async-done | bytes 1048592 | tf_op jit(solution)/shard_map/all_gather | solution.py:103
  377.9 54.9 %all-gather.11.cloned.1.call-done = bf16[4096,512]{1,0:T(8,128)(2,1)} async-done(((bf16[1024,512]{1,0:T(8,128)(2,1)}), bf16[4096,512]{1,0:T(8,128)(2,1)}) %all-gather.11.cloned.1.call-update) | async-done | bytes 4194320 | tf_op jit(solution)/shard_map/all_gather | solution.py:104
  432.8 55.0 %all-gather.7.cloned.1.call-done = bf16[4096,512]{1,0:T(8,128)(2,1)} async-done(((bf16[1024,512]{1,0:T(8,128)(2,1)}), bf16[4096,512]{1,0:T(8,128)(2,1)}) %all-gather.7.cloned.1.call-update) | async-done | bytes 4194320 | tf_op jit(solution)/shard_map/all_gather | solution.py:102
  487.8 4.6 copy.40
  492.5 1.0 copy.41
  493.4 2.0 copy.42
  (36 shorter events, 0.1 us)
Async XLA Ops:
  7.2 87.2 %copy-start = (bf16[1024,512]{1,0:T(8,128)(2,1)S(1)}, bf16[1024,512]{1,0:T(8,128)(2,1)}, u32[]{:S(2)}) copy-start(bf16[1024,512]{1,0:T(8,128)(2,1)} %param.21) | copy-start | bytes 3145732
  7.2 87.2 %all-gather.5.cloned.1.call-start = ((), (), s32[]{:S(2)}) async-start(), calls=%async_computation.1 | async-start | bytes 9437184 | tf_op jit(solution)/shard_map/all_gather | solution.py:59
  7.9 181.9 %reduce-scatter.2.cloned.1.call-start = ((), (), s32[]{:S(2)}) async-start(), calls=%async_computation.2 | async-start | bytes 10485760 | tf_op jit(solution)/shard_map/reduce_scatter | solution.py:71
  104.9 1.2 copy-start.2
  104.9 150.9 %all-reduce.5.cloned.1.call-start = ((), (), s32[]{:S(2)}) async-start(), calls=%async_computation.6 | async-start | bytes 3145728 | tf_op jit(solution)/shard_map/psum | solution.py:62
  110.4 145.4 %copy-start.11 = (bf16[1024,512]{1,0:T(8,128)(2,1)S(1)}, bf16[1024,512]{1,0:T(8,128)(2,1)}, u32[]{:S(2)}) copy-start(bf16[1024,512]{1,0:T(8,128)(2,1)} %param.18) | copy-start | bytes 3145732
  193.3 65.0 %copy-start.19 = (bf16[1024,128]{1,0:T(8,128)(2,1)S(1)}, bf16[1024,128]{1,0:T(8,128)(2,1)}, u32[]{:S(2)}) copy-start(bf16[1024,128]{1,0:T(8,128)(2,1)} %param.19) | copy-start | bytes 786436
  193.3 153.5 %copy-start.20 = (f32[128,128]{1,0:T(8,128)S(1)}, f32[128,128]{1,0:T(8,128)}, u32[]{:S(2)}) copy-start(f32[128,128]{1,0:T(8,128)} %param.31) | copy-start | bytes 196612
  193.3 153.5 %copy-start.21 = (f32[128,128]{1,0:T(8,128)S(1)}, f32[128,128]{1,0:T(8,128)}, u32[]{:S(2)}) copy-start(f32[128,128]{1,0:T(8,128)} %param.30) | copy-start | bytes 196612
  193.3 109.0 %all-reduce.7.cloned.1.call-start = ((), (), s32[]{:S(2)}) async-start(), calls=%async_computation.7 | async-start | bytes 655360 | tf_op jit(solution)/shard_map/psum | solution.py:78
  255.8 2.5 copy-start.15
  255.8 3.6 copy-start.6
  255.8 91.9 %copy-start.14 = (f32[1024,128]{1,0:T(8,128)S(1)}, f32[1024,128]{1,0:T(8,128)}, u32[]{:S(2)}) copy-start(f32[1024,128]{1,0:T(8,128)} %param.23) | copy-start | bytes 1572868
  259.3 118.6 %all-gather.9.cloned.1.call-start = ((), (), s32[]{:S(2)}) async-start(), calls=%async_computation.4 | async-start | bytes 1310720 | tf_op jit(solution)/shard_map/all_gather | solution.py:103
  347.6 4.0 copy-start.17
  347.6 4.0 copy-start.18
  347.7 4.0 copy-start.7
  350.3 82.5 %all-gather.11.cloned.1.call-start = ((), (), s32[]{:S(2)}) async-start(), calls=%async_computation.5 | async-start | bytes 5242880 | tf_op jit(solution)/shard_map/all_gather | solution.py:104
  351.7 4.7 copy-start.4
  351.7 4.7 copy-start.5
  351.7 4.8 copy-start.12
  351.7 4.8 copy-start.16
  356.4 1.7 copy-start.8
  356.4 131.4 %all-gather.7.cloned.1.call-start = ((), (), s32[]{:S(2)}) async-start(), calls=%async_computation.3 | async-start | bytes 5242880 | tf_op jit(solution)/shard_map/all_gather | solution.py:102
  357.7 5.0 copy-start.9
  357.7 5.0 copy-start.10
  487.8 4.6 copy-start.13
  487.8 5.6 %copy-start.3 = (bf16[4096,512]{1,0:T(8,128)(2,1)S(1)}, bf16[4096,512]{1,0:T(8,128)(2,1)}, u32[]{:S(2)}) copy-start(bf16[4096,512]{1,0:T(8,128)(2,1)} %all-gather.11.cloned.1.call-done) | copy-start | bytes 12582916
  493.4 2.0 copy-start.1
Sparse Core Ops, SparseCore 0:
  9.6 84.7 all-gather.4
  105.0 84.7 reduce-scatter.1
  193.6 62.1 all-reduce.4
  259.4 42.8 all-reduce.6
  350.4 27.4 all-gather.8
  380.2 52.5 all-gather.10
  435.2 52.5 all-gather.6
where the time goes:
time: 503 us; the launch traced here: 502 us
  waiting for transfers between devices  396 us (79%)
  blocking collectives  39.3 us (8%)
  matrix products  33.4 us (7%)
  between operations  17 us (3%)
  local copies, waits for them, and re-layouts  9.28 us (2%)
  other arithmetic  7.2 us (1%)
    all_gather x1, waiting for transfers between devices, per_device(): whole_values = lax.all_gather(head_outputs, 'tp', axis=1, tiled=True)  86.4 us
    reduce_scatter x1, waiting for transfers between devices, per_device(): lax.psum_scatter(over_tokens(whole_values, branch_upstream), 'fs', scatte...  79.4 us
    psum x1, waiting for transfers between devices, per_device(): lax.psum((jnp.dot(normed_inputs, block_query, preferred_element_type=jnp....  62.4 us
    all_gather x1, waiting for transfers between devices, per_device(): lax.all_gather(query_updated.astype(jnp.bfloat16), 'fs', axis=0, tiled=True)  55 us
    all_gather x1, waiting for transfers between devices, per_device(): lax.all_gather(branch_updated.astype(jnp.bfloat16), 'fs', axis=0, tiled=T...  54.9 us
    psum x1, waiting for transfers between devices, per_device(): query_low, key_low = lax.psum((part_query, part_key), 'fs')  41.6 us
    psum x1, blocking collectives, per_device(): total = lax.psum(local_squares, ('fs', 'tp'))  39.3 us
    all_gather x1, waiting for transfers between devices, per_device(): lax.all_gather(key_updated.astype(jnp.bfloat16), 'fs', axis=0, tiled=True)  15.2 us
  transfers between devices with their start and end apart: 7, of which 7 were waited for; matrix products, arithmetic and copies ran while one was open for 3% of the time, Pallas kernels for 0%

commit v1 on v0

--- a/solution.py
+++ b/solution.py
@@ -79,7 +79,7 @@
     branch_low = lax.psum(part_branch, "tp")
     local_squares = (jnp.sum(query_low * query_low) + jnp.sum(key_low * key_low)) / n_rows
     local_squares = local_squares + jnp.sum(branch_low * branch_low) / n_cols
-    total = lax.psum(local_squares, ("fs", "tp"))
+    total = lax.psum(lax.psum(local_squares, "tp"), "fs")
     entries = rank * n_cols * (2 * query_local + key_local)
     rms_value = jnp.sqrt(total / float(entries))
     clip = 1.0 / jnp.maximum(1.0, rms_value / CLIP_RMS)

time: 503 us -> 486 us (0.966)
  blocking collectives: 39.3 us -> 25.9 us
    psum x1 -> x2, blocking collectives: 39.3 us -> 25.9 us  [per_device(): total = lax.psum(lax.psum(local_squares, 'tp'), 'fs')]
where the time goes in v1:
time: 486 us; the launch traced here: 485 us
  waiting for transfers between devices  392 us (81%)
  matrix products  33.4 us (7%)
  blocking collectives  25.9 us (5%)
  between operations  17 us (3%)
  local copies, waits for them, and re-layouts  9.24 us (2%)
  other arithmetic  7.2 us (1%)
    all_gather x1, waiting for transfers between devices, per_device(): whole_values = lax.all_gather(head_outputs, 'tp', axis=1, tiled=True)  86.4 us
    reduce_scatter x1, waiting for transfers between devices, per_device(): lax.psum_scatter(over_tokens(whole_values, branch_upstream), 'fs', scatte...  79.4 us
    psum x1, waiting for transfers between devices, per_device(): lax.psum((jnp.dot(normed_inputs, block_query, preferred_element_type=jnp....  62.4 us
    all_gather x1, waiting for transfers between devices, per_device(): lax.all_gather(query_updated.astype(jnp.bfloat16), 'fs', axis=0, tiled=True)  55 us
    all_gather x1, waiting for transfers between devices, per_device(): lax.all_gather(branch_updated.astype(jnp.bfloat16), 'fs', axis=0, tiled=T...  54.9 us
    psum x1, waiting for transfers between devices, per_device(): query_low, key_low = lax.psum((part_query, part_key), 'fs')  41.6 us
    psum x2, blocking collectives, per_device(): total = lax.psum(lax.psum(local_squares, 'tp'), 'fs')  25.9 us
    dot_general x3, matrix products, over_tokens(): lax.dot_general(left, right, (((0,), (0,)), ((), ())), precision=precisio...  13.9 us
  transfers between devices with their start and end apart: 7, of which 7 were waited for; matrix products, arithmetic and copies ran while one was open for 3% of the time, Pallas kernels for 0%

profile of v1, /device:TPU:0, one launch (start us, length us, event | category | flops | bytes accessed | tf_op | source)
XLA Modules:
  0.0 485.1 jit_solution(5154986880827905871)
XLA Ops:
  7.2 0.0 copy-start
  7.2 0.0 all-gather.5.cloned.1.call-start
  7.2 0.7 all-gather.5.cloned.1.call-update
  7.9 0.0 reduce-scatter.2.cloned.1.call-start
  8.0 86.4 %all-gather.5.cloned.1.call-done = bf16[1024,4096]{1,0:T(8,128)(2,1)} async-done(((bf16[1024,512]{1,0:T(8,128)(2,1)}), bf16[1024,4096]{1,0:T(8,128)(2,1)}) %all-gather.5.cloned.1.call-update) | async-done | bytes 8388624 | tf_op jit(solution)/shard_map/all_gather | solution.py:59
  94.4 10.5 %fusion.39 = f32[4096,512]{1,0:T(8,128)} fusion(bf16[1024,4096]{1,0:T(8,128)(2,1)} %all-gather.5.cloned.1.call-done, bf16[1024,512]{1,0:T(8,128)(2,1)S(1)} %copy-done), kind=kOutput, calls=%fused_computation.53 | convolution fusion | flops 4294967296 | bytes 17825792 | tf_op jit(solution)/shard_map/dot_general | solution.py:21
  104.9 0.0 reduce-scatter.2.cloned.1.call-update
  104.9 0.0 all-reduce.5.cloned.1.call-start
  104.9 1.1 copy-done.2
  106.1 2.2 convolution_bitcast_fusion
  108.3 2.2 convolution_bitcast_fusion.1
  110.4 79.4 %reduce-scatter.2.cloned.1.call-done = f32[1024,512]{1,0:T(8,128)} async-done(((f32[4096,512]{1,0:T(8,128)}), f32[1024,512]{1,0:T(8,128)}) %reduce-scatter.2.cloned.1.call-update) | async-done | bytes 2097168 | tf_op jit(solution)/shard_map/reduce_scatter | solution.py:71
  189.8 3.4 fusion.18
  193.3 0.0 all-reduce.5.cloned.1.call-update
  193.3 0.0 all-reduce.7.cloned.1.call-start
  193.4 62.4 %all-reduce.5.cloned.1.call-done = (f32[1024,128]{0,1:T(8,128)}, f32[1024,128]{0,1:T(8,128)}, f32[1024,128]{1,0:T(8,128)}) async-done(((f32[1024,128]{0,1:T(8,128)}, f32[1024,128]{0,1:T(8,128)}, f32[1024,128]{1,0:T(8,128)}), (f32[1024,128]{0,1:T(8,128)}, f32[1024,128]{0,1:T(8,128)}, f32[1024,128]{1,0:T(8,128)})) %all-reduce.5.cloned.1.call-update) | async-done | bytes 1572880 | tf_op jit(solution)/shard_map/psum | solution.py:62
  255.8 2.5 fusion.37
  258.3 1.0 fusion.38
  259.3 0.0 all-reduce.7.cloned.1.call-update
  259.3 0.0 all-gather.9.cloned.1.call-start
  259.4 0.7 multiply_reduce_fusion
  260.8 41.6 %all-reduce.7.cloned.1.call-done = (f32[128,512]{1,0:T(8,128)}, f32[128,128]{1,0:T(8,128)}) async-done(((f32[128,512]{1,0:T(8,128)}, f32[128,128]{1,0:T(8,128)}), (f32[128,512]{1,0:T(8,128)}, f32[128,128]{1,0:T(8,128)})) %all-reduce.7.cloned.1.call-update) | async-done | bytes 327696 | tf_op jit(solution)/shard_map/psum | solution.py:78
  302.3 1.6 multiply_reduce_fusion.1
  303.9 1.5 multiply_reduce_fusion.2
  306.7 16.4 %psum.54 = f32[]{:T(128)} all-reduce(f32[]{:T(128)S(6)} %add.70), channel_id=1, replica_groups=mesh['fs'=4,'tp'=8] {'tp'}, use_global_device_ids=true, to_apply=%region_9.0 | all-reduce | flops 1 | bytes 8 | tf_op jit(solution)/shard_map/psum | solution.py:82
  323.1 9.5 %psum.55 = f32[]{:T(128)} all-reduce(f32[]{:T(128)} %psum.54), channel_id=1, replica_groups=mesh['fs'=4,'tp'=8] {'fs'}, use_global_device_ids=true, to_apply=%region_10.0 | all-reduce | flops 1 | bytes 8 | tf_op jit(solution)/shard_map/psum | solution.py:82
  333.4 0.9 fusion.20
  334.3 2.6 fusion.35
  336.8 0.0 all-gather.9.cloned.1.call-update
  336.8 0.0 all-gather.11.cloned.1.call-start
  336.9 1.4 fusion
  338.3 0.0 copy-start.4
  338.3 0.0 copy-start.5
  338.3 4.7 fusion.34
  343.0 0.0 all-gather.11.cloned.1.call-update
  343.0 0.0 all-gather.7.cloned.1.call-start
  343.1 1.2 fusion.5
  344.3 0.0 copy-start.9
  344.3 0.0 copy-start.10
  344.3 0.4 copy-done.8
  344.7 4.5 fusion.36
  349.2 0.0 all-gather.7.cloned.1.call-update
  349.2 11.5 %all-gather.9.cloned.1.call-done = bf16[4096,128]{1,0:T(8,128)(2,1)} async-done(((bf16[1024,128]{1,0:T(8,128)(2,1)}), bf16[4096,128]{1,0:T(8,128)(2,1)}) %all-gather.9.cloned.1.call-update) | async-done | bytes 1048592 | tf_op jit(solution)/shard_map/all_gather | solution.py:103
  360.7 54.9 %all-gather.11.cloned.1.call-done = bf16[4096,512]{1,0:T(8,128)(2,1)} async-done(((bf16[1024,512]{1,0:T(8,128)(2,1)}), bf16[4096,512]{1,0:T(8,128)(2,1)}) %all-gather.11.cloned.1.call-update) | async-done | bytes 4194320 | tf_op jit(solution)/shard_map/all_gather | solution.py:104
  415.6 55.0 %all-gather.7.cloned.1.call-done = bf16[4096,512]{1,0:T(8,128)(2,1)} async-done(((bf16[1024,512]{1,0:T(8,128)(2,1)}), bf16[4096,512]{1,0:T(8,128)(2,1)}) %all-gather.7.cloned.1.call-update) | async-done | bytes 4194320 | tf_op jit(solution)/shard_map/all_gather | solution.py:102
  470.6 4.6 copy.40
  475.3 1.0 copy.41
  476.2 2.0 copy.42
  (37 shorter events, 0.1 us)
Async XLA Ops:
  7.2 87.2 %copy-start = (bf16[1024,512]{1,0:T(8,128)(2,1)S(1)}, bf16[1024,512]{1,0:T(8,128)(2,1)}, u32[]{:S(2)}) copy-start(bf16[1024,512]{1,0:T(8,128)(2,1)} %param.21) | copy-start | bytes 3145732
  7.2 87.2 %all-gather.5.cloned.1.call-start = ((), (), s32[]{:S(2)}) async-start(), calls=%async_computation.1 | async-start | bytes 9437184 | tf_op jit(solution)/shard_map/all_gather | solution.py:59
  7.9 181.9 %reduce-scatter.2.cloned.1.call-start = ((), (), s32[]{:S(2)}) async-start(), calls=%async_computation.2 | async-start | bytes 10485760 | tf_op jit(solution)/shard_map/reduce_scatter | solution.py:71
  104.9 1.2 copy-start.2
  104.9 150.9 %all-reduce.5.cloned.1.call-start = ((), (), s32[]{:S(2)}) async-start(), calls=%async_computation.6 | async-start | bytes 3145728 | tf_op jit(solution)/shard_map/psum | solution.py:62
  110.4 145.4 %copy-start.11 = (bf16[1024,512]{1,0:T(8,128)(2,1)S(1)}, bf16[1024,512]{1,0:T(8,128)(2,1)}, u32[]{:S(2)}) copy-start(bf16[1024,512]{1,0:T(8,128)(2,1)} %param.18) | copy-start | bytes 3145732
  193.3 65.0 %copy-start.19 = (bf16[1024,128]{1,0:T(8,128)(2,1)S(1)}, bf16[1024,128]{1,0:T(8,128)(2,1)}, u32[]{:S(2)}) copy-start(bf16[1024,128]{1,0:T(8,128)(2,1)} %param.19) | copy-start | bytes 786436
  193.3 140.0 %copy-start.20 = (f32[128,128]{1,0:T(8,128)S(1)}, f32[128,128]{1,0:T(8,128)}, u32[]{:S(2)}) copy-start(f32[128,128]{1,0:T(8,128)} %param.31) | copy-start | bytes 196612
  193.3 140.0 %copy-start.21 = (f32[128,128]{1,0:T(8,128)S(1)}, f32[128,128]{1,0:T(8,128)}, u32[]{:S(2)}) copy-start(f32[128,128]{1,0:T(8,128)} %param.30) | copy-start | bytes 196612
  193.3 109.0 %all-reduce.7.cloned.1.call-start = ((), (), s32[]{:S(2)}) async-start(), calls=%async_computation.7 | async-start | bytes 655360 | tf_op jit(solution)/shard_map/psum | solution.py:78
  255.8 2.5 copy-start.15
  255.8 3.6 copy-start.6
  255.8 78.4 %copy-start.14 = (f32[1024,128]{1,0:T(8,128)S(1)}, f32[1024,128]{1,0:T(8,128)}, u32[]{:S(2)}) copy-start(f32[1024,128]{1,0:T(8,128)} %param.23) | copy-start | bytes 1572868
  259.3 101.4 %all-gather.9.cloned.1.call-start = ((), (), s32[]{:S(2)}) async-start(), calls=%async_computation.4 | async-start | bytes 1310720 | tf_op jit(solution)/shard_map/all_gather | solution.py:103
  334.2 4.0 copy-start.17
  334.2 4.0 copy-start.18
  334.3 4.0 copy-start.7
  336.8 78.7 %all-gather.11.cloned.1.call-start = ((), (), s32[]{:S(2)}) async-start(), calls=%async_computation.5 | async-start | bytes 5242880 | tf_op jit(solution)/shard_map/all_gather | solution.py:104
  338.3 4.7 copy-start.4
  338.3 4.7 copy-start.5
  338.3 4.8 copy-start.12
  338.3 4.8 copy-start.16
  343.0 1.7 copy-start.8
  343.0 127.6 %all-gather.7.cloned.1.call-start = ((), (), s32[]{:S(2)}) async-start(), calls=%async_computation.3 | async-start | bytes 5242880 | tf_op jit(solution)/shard_map/all_gather | solution.py:102
  344.3 4.9 %copy-start.9 = (f32[128,512]{1,0:T(8,128)}, f32[128,512]{1,0:T(8,128)S(1)}, u32[]{:S(2)}) copy-start(f32[128,512]{1,0:T(8,128)S(1)} %get-tuple-element.60) | copy-start | bytes 786436
  344.3 4.9 %copy-start.10 = (f32[128,512]{1,0:T(8,128)}, f32[128,512]{1,0:T(8,128)S(1)}, u32[]{:S(2)}) copy-start(f32[128,512]{1,0:T(8,128)S(1)} %get-tuple-element.59) | copy-start | bytes 786436
  470.6 4.6 copy-start.13
  470.6 5.6 %copy-start.3 = (bf16[4096,512]{1,0:T(8,128)(2,1)S(1)}, bf16[4096,512]{1,0:T(8,128)(2,1)}, u32[]{:S(2)}) copy-start(bf16[4096,512]{1,0:T(8,128)(2,1)} %all-gather.11.cloned.1.call-done) | copy-start | bytes 12582916
  476.2 2.0 copy-start.1
Sparse Core Ops, SparseCore 0:
  9.6 84.7 all-gather.4
  105.0 84.7 reduce-scatter.1
  193.6 62.1 all-reduce.4
  259.4 42.8 all-reduce.6
  337.0 23.6 all-gather.8
  363.0 52.5 all-gather.10
  418.0 52.5 all-gather.6
